TPU v7x, 32 devices: a whole 2x2x4 slice. The times are simulated.
32 devices in a mesh: fs: 8 (over z, core), tp: 4 (over y, x).
Axes of the slice: x: 2, y: 2, z: 4, core: 2. Of those that a mesh axis runs over, the one named last changes fastest.
Arguments:
- tokens: bfloat16 [4096, 4096], P('fs', 'tp'), may hold values from -16 to 16
- norm_gain: float32 [4096], P('fs'), may hold values from 0.1 to 1.9
- gate_train: float32 [4096, 12288], P('fs', 'tp'), may hold values from -6 to 6
- up_train: float32 [4096, 12288], P('fs', 'tp'), may hold values from -6 to 6
Outputs:
- gate_serve: bfloat16 [4096, 12288], P(None, 'tp')
- up_serve: bfloat16 [4096, 12288], P(None, 'tp')
- hidden: bfloat16 [4096, 12288], P('fs', 'tp')
All inputs are finite; a program needn't handle non-finite values.
Results may differ from a plain program's by a relative error of at most 0.0071.
Values may be sent and summed in bfloat16 or wider, within the bound.
A program may use at most 192 MiB of HBM per device.

v0:
```python
import jax
import jax.numpy as jnp
from jax import lax
from jax.sharding import PartitionSpec as P


def body(tokens, norm_gain, gate_train, up_train):
    gain = norm_gain[:, None]
    gate_local = (gate_train * gain).astype(jnp.bfloat16)
    up_local = (up_train * gain).astype(jnp.bfloat16)
    whole = lax.all_gather(tokens, "tp", axis=1, tiled=True)
    values = whole.astype(jnp.float32)
    normed = (values * lax.rsqrt(jnp.mean(values * values, axis=-1, keepdims=True) + 1e-06)).astype(
        jnp.bfloat16
    )
    width = normed.shape[1]
    scale = width ** (-0.5)
    gate_serve, up_serve = (
        lax.all_gather(gate_local, "fs", axis=0, tiled=True),
        lax.all_gather(up_local, "fs", axis=0, tiled=True),
    )
    gate_acc = jnp.dot(normed, gate_serve, preferred_element_type=jnp.float32)
    up_acc = jnp.dot(normed, up_serve, preferred_element_type=jnp.float32)
    gate = gate_acc * scale
    up = up_acc * scale
    hidden = (jax.nn.silu(gate) * up).astype(jnp.bfloat16)
    return (gate_serve, up_serve, hidden)


def solution(mesh):
    in_specs = (P("fs", "tp"), P("fs"), P("fs", "tp"), P("fs", "tp"))
    out_specs = (P(None, "tp"), P(None, "tp"), P("fs", "tp"))
    return jax.shard_map(body, mesh=mesh, in_specs=in_specs, out_specs=out_specs, check_vma=False)
```

profile of v0, /device:TPU:0, one launch (start us, length us, event | category | flops | bytes accessed | tf_op | source)
XLA Modules:
  0.0 569.7 jit_solution(12411793271498854987)
XLA Ops:
  7.2 0.0 all-gather.8.cloned.1.call-start
  7.2 0.7 all-gather.8.cloned.1.call-update
  7.9 0.0 all-gather.4.cloned.1.call-start
  7.9 9.3 %multiply_convert_fusion.1 = (bf16[512,3072]{1,0:T(8,128)(2,1)}, bf16[512,3072]{1,0:T(8,128)(2,1)}) fusion(f32[512,3072]{1,0:T(8,128)} %param.7, f32[512]{0:T(512)} %param.5, f32[512,3072]{1,0:T(8,128)} %param.6), kind=kLoop, calls=%fused_computation.5 | loop fusion | flops 6291456 | bytes 18876416 | tf_op jit(solution)/shard_map/convert_element_type | solution.py:10
  17.2 0.0 all-gather.4.cloned.1.call-update
  17.3 0.0 all-gather.6.cloned.1.call-start
  17.3 0.7 all-gather.6.cloned.1.call-update
  18.0 47.2 %all-gather.8.cloned.1.call-done = bf16[512,4096]{1,0:T(8,128)(2,1)} async-done(((bf16[512,1024]{1,0:T(8,128)(2,1)}), bf16[512,4096]{1,0:T(8,128)(2,1)}) %all-gather.8.cloned.1.call-update) | async-done | bytes 4194320 | tf_op jit(solution)/shard_map/all_gather | solution.py:11
  65.1 3.1 fusion
  68.2 219.0 %all-gather.4.cloned.1.call-done = bf16[4096,3072]{1,0:T(8,128)(2,1)} async-done(((bf16[512,3072]{1,0:T(8,128)(2,1)}), bf16[4096,3072]{1,0:T(8,128)(2,1)}) %all-gather.4.cloned.1.call-update) | async-done | bytes 25165840 | tf_op jit(solution)/shard_map/all_gather | solution.py:19
  287.2 20.6 %fusion.3 = f32[512,3072]{1,0:T(8,128)} fusion(bf16[4096,3072]{1,0:T(8,128)(2,1)} %all-gather.4.cloned.1.call-done, bf16[512,4096]{1,0:T(8,128)(2,1)} %all-gather.8.cloned.1.call-done, f32[512]{0:T(512)S(1)} %add_rsqrt_fusion), kind=kOutput, calls=%fused_computation.7 | convolution fusion | flops 12891193344 | bytes 35653632 | tf_op jit(solution)/shard_map/dot_general | solution.py:22
  307.8 199.7 %all-gather.6.cloned.1.call-done = bf16[4096,3072]{1,0:T(8,128)(2,1)} async-done(((bf16[512,3072]{1,0:T(8,128)(2,1)}), bf16[4096,3072]{1,0:T(8,128)(2,1)}) %all-gather.6.cloned.1.call-update) | async-done | bytes 25165840 | tf_op jit(solution)/shard_map/all_gather | solution.py:20
  507.5 21.8 %multiply_convert_fusion = bf16[512,3072]{1,0:T(8,128)(2,1)} fusion(f32[512,3072]{1,0:T(8,128)} %fusion.3, bf16[4096,3072]{1,0:T(8,128)(2,1)} %all-gather.6.cloned.1.call-done, bf16[512,4096]{1,0:T(8,128)(2,1)} %all-gather.8.cloned.1.call-done, f32[512]{0:T(512)S(1)} %add_rsqrt_fusion), kind=kOutput, calls=%fused_computation.4 | convolution fusion | flops 12903776256 | bytes 38799360 | tf_op jit(solution)/shard_map/dot_general | solution.py:23
  529.4 0.0 copy-start
  529.4 22.0 %copy.9 = bf16[4096,3072]{1,0:T(8,128)(2,1)} copy(bf16[4096,3072]{1,0:T(8,128)(2,1)} %all-gather.4.cloned.1.call-done) | data formatting | bytes 50331648
  551.3 2.9 copy-done
  554.3 8.9 %copy.10 = bf16[4096,3072]{1,0:T(8,128)(2,1)} copy(bf16[4096,3072]{1,0:T(8,128)(2,1)S(1)} %copy-done) | data formatting | bytes 50331648
  (1 shorter events, 0.0 us)
Async XLA Ops:
  7.2 58.0 %all-gather.8.cloned.1.call-start = ((), (), s32[]{:S(2)}) async-start(), calls=%async_computation.2 | async-start | bytes 5242880 | tf_op jit(solution)/shard_map/all_gather | solution.py:11
  7.9 279.3 %all-gather.4.cloned.1.call-start = ((), (), s32[]{:S(2)}) async-start(), calls=%async_computation | async-start | bytes 28311552 | tf_op jit(solution)/shard_map/all_gather | solution.py:19
  17.3 490.3 %all-gather.6.cloned.1.call-start = ((), (), s32[]{:S(2)}) async-start(), calls=%async_computation.1 | async-start | bytes 28311552 | tf_op jit(solution)/shard_map/all_gather | solution.py:20
  529.4 24.9 %copy-start = (bf16[4096,3072]{1,0:T(8,128)(2,1)S(1)}, bf16[4096,3072]{1,0:T(8,128)(2,1)}, u32[]{:S(2)}) copy-start(bf16[4096,3072]{1,0:T(8,128)(2,1)} %all-gather.6.cloned.1.call-done) | copy-start | bytes 75497472
Sparse Core Ops, SparseCore 0:
  9.8 55.2 all-gather.7
  67.4 219.8 all-gather.3
  289.5 218.0 all-gather.5
where the time goes:
time: 570 us
  waiting for transfers between devices  467 us (82%)
  matrix products  42.4 us (7%)
  local copies, waits for them, and re-layouts  33.8 us (6%)
  between operations  13.7 us (2%)
  other arithmetic  12.4 us (2%)
    all_gather x1, waiting for transfers between devices, body(): lax.all_gather(gate_local, 'fs', axis=0, tiled=True)  219 us
    all_gather x1, waiting for transfers between devices, body(): lax.all_gather(up_local, 'fs', axis=0, tiled=True)  200 us
    all_gather x1, waiting for transfers between devices, body(): whole = lax.all_gather(tokens, 'tp', axis=1, tiled=True)  47.2 us
    unnamed x4, local copies, waits for them, and re-layouts  33.8 us
    dot_general x1, matrix products, body(): up_acc = jnp.dot(normed, up_serve, preferred_element_type=jnp.float32)  21.8 us
    dot_general x1, matrix products, body(): gate_acc = jnp.dot(normed, gate_serve, preferred_element_type=jnp.float32)  20.6 us
  transfers between devices with their start and end apart: 3, of which 3 were waited for; matrix products, arithmetic and copies ran while one was open for 6% of the time, Pallas kernels for 0%

commit v1 on v0

--- a/solution.py
+++ b/solution.py
@@ -16,7 +16,9 @@
     width = normed.shape[1]
     scale = width ** (-0.5)
     gate_serve, up_serve = (
-        lax.all_gather(gate_local, "fs", axis=0, tiled=True),
+        jnp.concatenate(
+            lax.all_to_all(jnp.stack([gate_local] * lax.axis_size("fs")), "fs", 0, 0), axis=0
+        ),
         lax.all_gather(up_local, "fs", axis=0, tiled=True),
     )
     gate_acc = jnp.dot(normed, gate_serve, preferred_element_type=jnp.float32)

time: 570 us -> 861 us (1.51)
  waiting for transfers between devices: 467 us -> 744 us
  local copies, waits for them, and re-layouts: 33.8 us -> 42.9 us
    all_to_all x0 -> x1, waiting for transfers between devices: none -> 710 us  [body(): lax.all_to_all(jnp.stack([gate_local] * lax.axis_size('fs')), 'fs', 0, 0)]
    all_gather x1 -> x0, waiting for transfers between devices: 219 us -> none  [body(): lax.all_gather(gate_local, 'fs', axis=0, tiled=True)]
    all_gather x1, waiting for transfers between devices: 200 us -> 0.01 us  [body(): lax.all_gather(up_local, 'fs', axis=0, tiled=True)]
    all_gather x1, waiting for transfers between devices: 47.2 us -> 32.8 us  [body(): whole = lax.all_gather(tokens, 'tp', axis=1, tiled=True)]
    another operation x0 -> x1, local copies, waits for them, and re-layouts: none -> 9.05 us  [body(): jnp.stack([gate_local] * lax.axis_size('fs'))]
  transfers between devices with their start and end apart: 3 -> 3, of which waited for: 3 -> 2; matrix products, arithmetic and copies ran while one was open for 6% -> 5% of each run, Pallas kernels for 0% -> 0%
where the time goes in v1:
time: 861 us; the launch traced here: 860 us
  waiting for transfers between devices  744 us (86%)
  local copies, waits for them, and re-layouts  42.9 us (5%)
  matrix products  41.5 us (5%)
  between operations  14.1 us (2%)
  other arithmetic  11.3 us (1%)
    all_to_all x1, waiting for transfers between devices, body(): lax.all_to_all(jnp.stack([gate_local] * lax.axis_size('fs')), 'fs', 0, 0)  710 us
    unnamed x4, local copies, waits for them, and re-layouts  33.8 us
    all_gather x1, waiting for transfers between devices, body(): whole = lax.all_gather(tokens, 'tp', axis=1, tiled=True)  32.8 us
    dot_general x1, matrix products, body(): up_acc = jnp.dot(normed, up_serve, preferred_element_type=jnp.float32)  22 us
    dot_general x1, matrix products, body(): gate_acc = jnp.dot(normed, gate_serve, preferred_element_type=jnp.float32)  19.5 us
  transfers between devices with their start and end apart: 3, of which 2 were waited for; matrix products, arithmetic and copies ran while one was open for 5% of the time, Pallas kernels for 0%

profile of v1, /device:TPU:0, one launch (start us, length us, event | category | flops | bytes accessed | tf_op | source)
XLA Modules:
  0.0 860.3 jit_solution(1921243299904565065)
XLA Ops:
  7.2 0.0 all-gather.5.cloned.1.call-start
  7.2 0.7 all-gather.5.cloned.1.call-update
  7.9 8.2 multiply_convert_fusion.1
  16.1 9.1 %stack.2 = bf16[8,512,3072]{2,1,0:T(8,128)(2,1)} broadcast(bf16[512,3072]{1,0:T(8,128)(2,1)S(1)} %get-tuple-element.4), dimensions={1,2} | broadcast | bytes 28311552 | tf_op jit(solution)/shard_map/stack | solution.py:20
  25.2 6.4 all-to-all-start
  31.6 0.0 all-gather.3.cloned.1.call-start
  31.7 0.7 all-gather.3.cloned.1.call-update
  32.4 32.8 %all-gather.5.cloned.1.call-done = bf16[512,4096]{1,0:T(8,128)(2,1)} async-done(((bf16[512,1024]{1,0:T(8,128)(2,1)}), bf16[512,4096]{1,0:T(8,128)(2,1)}) %all-gather.5.cloned.1.call-update) | async-done | bytes 4194320 | tf_op jit(solution)/shard_map/all_gather | solution.py:11
  65.1 3.1 fusion
  68.2 709.9 %all-to-all-done = bf16[8,512,3072]{2,1,0:T(8,128)(2,1)} async-done(((bf16[8,512,3072]{2,1,0:T(8,128)(2,1)}), bf16[8,512,3072]{2,1,0:T(8,128)(2,1)}, u32[]{:S(2)}, u32[]{:S(2)}) %all-to-all-start) | async-done | bytes 25165856 | tf_op jit(solution)/shard_map/all_to_all | solution.py:20
  778.1 19.5 %fusion.3 = f32[512,3072]{1,0:T(8,128)} fusion(bf16[4096,3072]{1,0:T(8,128)(2,1)} %bitcast, bf16[512,4096]{1,0:T(8,128)(2,1)} %all-gather.5.cloned.1.call-done, f32[512]{0:T(512)S(1)} %add_rsqrt_fusion), kind=kOutput, calls=%fused_computation.7 | convolution fusion | flops 12891193344 | bytes 35653632 | tf_op jit(solution)/shard_map/dot_general | solution.py:24
  797.6 0.0 all-gather.3.cloned.1.call-done
  797.6 22.0 %multiply_convert_fusion = bf16[512,3072]{1,0:T(8,128)(2,1)} fusion(f32[512,3072]{1,0:T(8,128)} %fusion.3, bf16[4096,3072]{1,0:T(8,128)(2,1)} %all-gather.3.cloned.1.call-done, bf16[512,4096]{1,0:T(8,128)(2,1)} %all-gather.5.cloned.1.call-done, f32[512]{0:T(512)S(1)} %add_rsqrt_fusion), kind=kOutput, calls=%fused_computation.4 | convolution fusion | flops 12903776256 | bytes 38799360 | tf_op jit(solution)/shard_map/dot_general | solution.py:25
  819.6 0.0 copy-start
  819.6 22.0 %copy.9 = bf16[4096,3072]{1,0:T(8,128)(2,1)} copy(bf16[4096,3072]{1,0:T(8,128)(2,1)} %bitcast) | data formatting | bytes 50331648
  841.6 2.9 copy-done
  844.5 8.9 %copy.10 = bf16[4096,3072]{1,0:T(8,128)(2,1)} copy(bf16[4096,3072]{1,0:T(8,128)(2,1)S(1)} %copy-done) | data formatting | bytes 50331648
  (1 shorter events, 0.0 us)
Async XLA Ops:
  7.2 58.0 %all-gather.5.cloned.1.call-start = ((), (), s32[]{:S(2)}) async-start(), calls=%async_computation.2 | async-start | bytes 5242880 | tf_op jit(solution)/shard_map/all_gather | solution.py:11
  25.2 752.9 %all-to-all-start = ((bf16[8,512,3072]{2,1,0:T(8,128)(2,1)}), bf16[8,512,3072]{2,1,0:T(8,128)(2,1)}, u32[]{:S(2)}, u32[]{:S(2)}) async-start(bf16[8,512,3072]{2,1,0:T(8,128)(2,1)} %stack.2), calls=%async_computation | async-start | bytes 50331648 | tf_op jit(solution)/shard_map/all_to_all | solution.py:20
  31.6 766.0 %all-gather.3.cloned.1.call-start = ((), (), s32[]{:S(2)}) async-start(), calls=%async_computation.1 | async-start | bytes 28311552 | tf_op jit(solution)/shard_map/all_gather | solution.py:22
  819.6 24.9 %copy-start = (bf16[4096,3072]{1,0:T(8,128)(2,1)S(1)}, bf16[4096,3072]{1,0:T(8,128)(2,1)}, u32[]{:S(2)}) copy-start(bf16[4096,3072]{1,0:T(8,128)(2,1)} %all-gather.3.cloned.1.call-done) | copy-start | bytes 75497472
Sparse Core Ops, SparseCore 0:
  9.8 55.2 all-gather.4
  67.4 438.7 all-gather.2
